TPU v7x, 32 devices: a whole 2x2x4 slice. The times are simulated.
32 devices in a mesh: sp: 4 (over y, x), tp: 8 (over z, core).
Axes of the slice: x: 2, y: 2, z: 4, core: 2. Of those that a mesh axis runs over, the one named last changes fastest.
Arguments:
- stream: bfloat16 [4096, 1024], P('tp', 'sp'), may hold values from -6 to 6
- value_weight: bfloat16 [2, 2048, 4096], P(None, 'tp', 'sp'), may hold values from -0.09375 to 0.09375
- gate_weight: bfloat16 [2, 2048, 4096], P(None, 'tp', 'sp'), may hold values from -0.09375 to 0.09375
- conv_taps: bfloat16 [2, 2048, 31], P(None, 'tp'), may hold values from -16 to 16
- norm_gain: bfloat16 [2, 2048], P(None, 'tp'), may hold values from 0.099609375 to 1.8984375
- out_weight: bfloat16 [2, 4096, 2048], P(None, 'tp', 'sp'), may hold values from -4 to 4
- out_gain: bfloat16 [2, 4096], P(None, 'tp'), may hold values from 0.099609375 to 1.8984375
Outputs:
- result: bfloat16 [4096, 1024], P('tp', 'sp')
All inputs are finite; a program needn't handle non-finite values.
Results may differ from a plain program's by a relative error of at most 0.015.
Values may be sent and summed in bfloat16 or wider, within the bound.
A program may use at most 64 MiB of HBM per device.

v0:
```python
import jax
import jax.numpy as jnp
from jax import lax
from jax.sharding import PartitionSpec as P

D = 4096
W = 2048
LAYERS = 2


def with_halo(cells, sides, width):
    for axis, dim in sides:
        count = lax.axis_size(axis)
        ends = count - 1
        head = lax.slice_in_dim(cells, 0, width, axis=dim)
        tail = lax.slice_in_dim(cells, cells.shape[dim] - width, cells.shape[dim], axis=dim)
        cells = jnp.concatenate(
            [
                lax.ppermute(tail, axis, [(i, (i + 1) % count) for i in range(ends)]),
                cells,
                lax.ppermute(head, axis, [((i + 1) % count, i) for i in range(ends)]),
            ],
            axis=dim,
        )
    return cells


def finish_layer(hidden, branch, feature_gain):
    branch_wide = lax.optimization_barrier(branch.astype(jnp.bfloat16)).astype(jnp.float32)
    square_total = lax.psum(jnp.sum(branch_wide * branch_wide, axis=0), "tp")
    factor = lax.rsqrt(square_total / D + 1e-06)
    return (hidden.astype(jnp.float32) + branch_wide * factor * feature_gain).astype(jnp.bfloat16)


def on_device(stream, value_weight, gate_weight, conv_taps, norm_gain, out_weight, out_gain):
    hidden = stream
    positions = hidden.shape[1]
    for layer_index in range(LAYERS):
        value_cols, gate_cols, out_cols = (
            lax.all_gather(value_weight[layer_index], "sp", axis=1, tiled=True),
            lax.all_gather(gate_weight[layer_index], "sp", axis=1, tiled=True),
            lax.all_gather(out_weight[layer_index], "sp", axis=1, tiled=True),
        )
        block_rows = lax.all_gather(hidden, "tp", axis=0, tiled=True)
        value_proj = jnp.dot(value_cols, block_rows, preferred_element_type=jnp.float32)
        gate_proj = jnp.dot(gate_cols, block_rows, preferred_element_type=jnp.float32)
        gated = (value_proj * jax.nn.sigmoid(gate_proj)).astype(jnp.bfloat16)
        kernel_taps = conv_taps[layer_index].astype(jnp.float32)
        reach = kernel_taps.shape[1] // 2
        padded = with_halo(gated, (("sp", 1),), reach).astype(jnp.float32)
        convolved = jnp.zeros(gated.shape, jnp.float32)
        for offset in range(kernel_taps.shape[1]):
            convolved = (
                convolved
                + kernel_taps[:, offset : offset + 1] * padded[:, offset : offset + positions]
            )
        conv_narrow = lax.optimization_barrier(convolved.astype(jnp.bfloat16))
        feature_gain = out_gain[layer_index].astype(jnp.float32)[:, None]
        conv_wide = conv_narrow.astype(jnp.float32)
        channel_totals = lax.psum(
            (jnp.sum(conv_wide, axis=0), jnp.sum(conv_wide * conv_wide, axis=0)), "tp"
        )
        average = channel_totals[0] / W
        variance = channel_totals[1] / W - average * average
        channel_gain = norm_gain[layer_index].astype(jnp.float32)[:, None]
        activated = jax.nn.silu(
            (conv_wide - average) * lax.rsqrt(variance + 1e-05) * channel_gain
        ).astype(jnp.bfloat16)
        branch = jnp.dot(
            out_cols,
            lax.all_gather(activated, "tp", axis=0, tiled=True),
            preferred_element_type=jnp.float32,
        )
        hidden = finish_layer(hidden, branch, feature_gain)
    return hidden


def solution(mesh):
    return jax.shard_map(
        on_device,
        mesh=mesh,
        in_specs=(
            P("tp", "sp"),
            P(None, "tp", "sp"),
            P(None, "tp", "sp"),
            P(None, "tp", None),
            P(None, "tp"),
            P(None, "tp", "sp"),
            P(None, "tp"),
        ),
        out_specs=P("tp", "sp"),
        check_vma=False,
    )
```

profile of v0, /device:TPU:0, one launch (start us, length us, event | category | flops | bytes accessed | tf_op | source)
XLA Modules:
  0.0 368.0 jit_solution(12427185381842521671)
XLA Ops:
  6.5 2.4 fusion.155
  9.7 1.0 fusion.154
  10.8 1.1 fusion.153
  12.1 35.0 %all-gather.27.cloned.1.call-done = bf16[1,256,4096]{2,1,0:T(8,128)(2,1)} async-done(((bf16[1,256,1024]{2,1,0:T(8,128)(2,1)}), bf16[1,256,4096]{2,1,0:T(8,128)(2,1)}) %all-gather.27.cloned.1.call-update) | async-done | bytes 2097168 | tf_op jit(solution)/shard_map/all_gather | solution.py:41
  47.1 30.8 %all-gather.17.cloned.1.call-done = bf16[4096,256]{1,0:T(8,128)(2,1)} async-done(((bf16[512,256]{1,0:T(8,128)(2,1)}), bf16[4096,256]{1,0:T(8,128)(2,1)}) %all-gather.17.cloned.1.call-update) | async-done | bytes 2097168 | tf_op jit(solution)/shard_map/all_gather | solution.py:44
  77.9 3.3 fusion.36
  81.2 33.1 %all-gather.25.cloned.1.call-done = bf16[1,256,4096]{2,1,0:T(8,128)(2,1)} async-done(((bf16[1,256,1024]{2,1,0:T(8,128)(2,1)}), bf16[1,256,4096]{2,1,0:T(8,128)(2,1)}) %all-gather.25.cloned.1.call-update) | async-done | bytes 2097168 | tf_op jit(solution)/shard_map/all_gather | solution.py:40
  114.4 2.5 fusion.57
  116.9 1.3 collective-permute-start.1
  118.2 4.5 %collective-permute-start = (bf16[256,15]{0,1:T(8,128)(2,1)S(1)}, bf16[256,15]{0,1:T(8,128)(2,1)S(1)}, u32[]{:S(2)}, u32[]{:S(2)}) collective-permute-start(bf16[256,15]{0,1:T(8,128)(2,1)S(1)} %get-tuple-element.21), channel_id=1, source_target_pairs={{0,8},{8,16},{16,24},{1,9},{9,17},{17,25},{2,10},{10,18},{18,26},{... | collective-permute-start | bytes 23048 | tf_op jit(solution)/shard_map/ppermute | solution.py:19
  122.8 1.3 collective-permute-done
  125.0 15.1 %all-reduce.1 = (f32[256]{0:T(256)S(1)}, f32[256]{0:T(256)S(1)}) all-reduce(f32[256]{0:T(256)S(1)} %get-tuple-element.8, f32[256]{0:T(256)S(1)} %get-tuple-element.7), channel_id=1, replica_groups=mesh['sp'=4,'tp'=8] {'tp'}, use_global_device_ids=true, to_apply=%region_3.0 | all-reduce | flops 512 | bytes 4096 | tf_op jit(solution)/shard_map/psum | solution.py:60
  140.1 0.8 fusion.78
  141.7 9.4 %all-gather.29.cloned.1.call-done = bf16[1,512,2048]{2,1,0:T(8,128)(2,1)} async-done(((bf16[1,512,512]{2,1,0:T(8,128)(2,1)}), bf16[1,512,2048]{2,1,0:T(8,128)(2,1)}) %all-gather.29.cloned.1.call-update) | async-done | bytes 2097168 | tf_op jit(solution)/shard_map/all_gather | solution.py:42
  151.1 25.3 %all-gather.19.cloned.1.call-done = bf16[2048,256]{0,1:T(8,128)(2,1)} async-done(((bf16[256,256]{0,1:T(8,128)(2,1)}), bf16[2048,256]{0,1:T(8,128)(2,1)}) %all-gather.19.cloned.1.call-update) | async-done | bytes 1048592 | tf_op jit(solution)/shard_map/all_gather | solution.py:71
  176.5 2.7 fusion.21
  179.3 15.7 %psum.44 = f32[256]{0:T(256)S(1)} all-reduce(f32[256]{0:T(256)S(1)} %fusion.63), channel_id=1, replica_groups=mesh['sp'=4,'tp'=8] {'tp'}, use_global_device_ids=true, to_apply=%region_5.6 | all-reduce | flops 256 | bytes 2048 | tf_op jit(solution)/shard_map/psum | solution.py:30
  195.0 0.9 fusion.66
  197.5 14.7 %all-gather.33.cloned.1.call-done = bf16[1,256,4096]{2,1,0:T(8,128)(2,1)} async-done(((bf16[1,256,1024]{2,1,0:T(8,128)(2,1)}), bf16[1,256,4096]{2,1,0:T(8,128)(2,1)}) %all-gather.33.cloned.1.call-update) | async-done | bytes 2097168 | tf_op jit(solution)/shard_map/all_gather | solution.py:41
  212.1 30.8 %all-gather.21.cloned.1.call-done = bf16[4096,256]{0,1:T(8,128)(2,1)} async-done(((bf16[512,256]{0,1:T(8,128)(2,1)}), bf16[4096,256]{0,1:T(8,128)(2,1)}) %all-gather.21.cloned.1.call-update) | async-done | bytes 2097168 | tf_op jit(solution)/shard_map/all_gather | solution.py:44
  242.9 3.1 fusion.51
  246.0 33.3 %all-gather.31.cloned.1.call-done = bf16[1,256,4096]{2,1,0:T(8,128)(2,1)} async-done(((bf16[1,256,1024]{2,1,0:T(8,128)(2,1)}), bf16[1,256,4096]{2,1,0:T(8,128)(2,1)}) %all-gather.31.cloned.1.call-update) | async-done | bytes 2097168 | tf_op jit(solution)/shard_map/all_gather | solution.py:40
  279.4 2.3 fusion.60
  281.7 1.3 collective-permute-start.3
  283.0 4.5 %collective-permute-start.2 = (bf16[256,15]{0,1:T(8,128)(2,1)S(1)}, bf16[256,15]{0,1:T(8,128)(2,1)S(1)}, u32[]{:S(2)}, u32[]{:S(2)}) collective-permute-start(bf16[256,15]{0,1:T(8,128)(2,1)S(1)} %get-tuple-element.19), channel_id=1, source_target_pairs={{0,8},{8,16},{16,24},{1,9},{9,17},{17,25},{2,10},{10,18},{18,26},{... | collective-permute-start | bytes 23048 | tf_op jit(solution)/shard_map/ppermute | solution.py:19
  287.6 1.3 collective-permute-done.2
  289.8 15.1 %all-reduce = (f32[256]{0:T(256)S(1)}, f32[256]{0:T(256)S(1)}) all-reduce(f32[256]{0:T(256)S(1)} %get-tuple-element.6, f32[256]{0:T(256)S(1)} %get-tuple-element.5), channel_id=1, replica_groups=mesh['sp'=4,'tp'=8] {'tp'}, use_global_device_ids=true, to_apply=%region_9.10 | all-reduce | flops 512 | bytes 4096 | tf_op jit(solution)/shard_map/psum | solution.py:60
  304.9 0.8 fusion.87
  305.7 10.5 %all-gather.35.cloned.1.call-done = bf16[1,512,2048]{2,1,0:T(8,128)(2,1)} async-done(((bf16[1,512,512]{2,1,0:T(8,128)(2,1)}), bf16[1,512,2048]{2,1,0:T(8,128)(2,1)}) %all-gather.35.cloned.1.call-update) | async-done | bytes 2097168 | tf_op jit(solution)/shard_map/all_gather | solution.py:42
  316.3 25.3 %all-gather.23.cloned.1.call-done = bf16[2048,256]{0,1:T(8,128)(2,1)} async-done(((bf16[256,256]{0,1:T(8,128)(2,1)}), bf16[2048,256]{0,1:T(8,128)(2,1)}) %all-gather.23.cloned.1.call-update) | async-done | bytes 1048592 | tf_op jit(solution)/shard_map/all_gather | solution.py:71
  341.6 2.7 fusion.18
  344.4 15.7 %psum.47 = f32[256]{0:T(256)S(1)} all-reduce(f32[256]{0:T(256)S(1)} %fusion.67), channel_id=1, replica_groups=mesh['sp'=4,'tp'=8] {'tp'}, use_global_device_ids=true, to_apply=%region_11.12 | all-reduce | flops 256 | bytes 2048 | tf_op jit(solution)/shard_map/psum | solution.py:30
  (65 shorter events, 6.4 us)
Async XLA Ops:
  6.5 3.2 copy-start.3
  6.5 40.6 %all-gather.27.cloned.1.call-start = ((), (), s32[]{:S(2)}) async-start(), calls=%async_computation.5 | async-start | bytes 2621440 | tf_op jit(solution)/shard_map/all_gather | solution.py:41
  8.9 1.9 copy-start.4
  8.9 69.0 %all-gather.17.cloned.1.call-start = ((), (), s32[]{:S(2)}) async-start(), calls=%async_computation | async-start | bytes 2359296 | tf_op jit(solution)/shard_map/all_gather | solution.py:44
  9.7 104.7 %all-gather.25.cloned.1.call-start = ((), (), s32[]{:S(2)}) async-start(), calls=%async_computation.4 | async-start | bytes 2621440 | tf_op jit(solution)/shard_map/all_gather | solution.py:40
  10.8 1.2 copy-start.6
  10.8 140.3 %all-gather.29.cloned.1.call-start = ((), (), s32[]{:S(2)}) async-start(), calls=%async_computation.6 | async-start | bytes 2621440 | tf_op jit(solution)/shard_map/all_gather | solution.py:42
  11.9 164.5 %all-gather.19.cloned.1.call-start = ((), (), s32[]{:S(2)}) async-start(), calls=%async_computation.1 | async-start | bytes 1179648 | tf_op jit(solution)/shard_map/all_gather | solution.py:71
  77.9 36.5 %copy-start.1 = (bf16[4096,256]{1,0:T(8,128)(2,1)S(1)}, bf16[4096,256]{1,0:T(8,128)(2,1)}, u32[]{:S(2)}) copy-start(bf16[4096,256]{1,0:T(8,128)(2,1)} %all-gather.17.cloned.1.call-done) | copy-start | bytes 6291460
  81.2 41.5 %copy-start.8 = (bf16[2,256]{1,0:T(2,128)(2,1)S(1)}, bf16[2,256]{1,0:T(2,128)(2,1)}, u32[]{:S(2)}) copy-start(bf16[2,256]{1,0:T(2,128)(2,1)} %param.11) | copy-start | bytes 3076
  116.9 5.9 %collective-permute-start.1 = (bf16[256,15]{0,1:T(8,128)(2,1)S(1)}, bf16[256,15]{0,1:T(8,128)(2,1)S(1)}, u32[]{:S(2)}, u32[]{:S(2)}) collective-permute-start(bf16[256,15]{0,1:T(8,128)(2,1)S(1)} %get-tuple-element.22), channel_id=1, source_target_pairs={{8,0},{16,8},{24,16},{9,1},{17,9},{25,17},{10,2},{18,10},{26,18},{... | collective-permute-start | bytes 23048 | tf_op jit(solution)/shard_map/ppermute | solution.py:21
  118.2 5.9 %collective-permute-start = (bf16[256,15]{0,1:T(8,128)(2,1)S(1)}, bf16[256,15]{0,1:T(8,128)(2,1)S(1)}, u32[]{:S(2)}, u32[]{:S(2)}) collective-permute-start(bf16[256,15]{0,1:T(8,128)(2,1)S(1)} %get-tuple-element.21), channel_id=1, source_target_pairs={{0,8},{8,16},{16,24},{1,9},{9,17},{17,25},{2,10},{10,18},{18,26},{... | collective-permute-start | bytes 23048 | tf_op jit(solution)/shard_map/ppermute | solution.py:19
  124.1 17.4 %copy-start.5 = (bf16[512,256]{1,0:T(8,128)(2,1)S(1)}, bf16[512,256]{1,0:T(8,128)(2,1)}, u32[]{:S(2)}) copy-start(bf16[512,256]{1,0:T(8,128)(2,1)} %param.7) | copy-start | bytes 786436
  124.1 17.6 %copy-start.7 = (bf16[2,512]{1,0:T(2,128)(2,1)S(1)}, bf16[2,512]{1,0:T(2,128)(2,1)}, u32[]{:S(2)}) copy-start(bf16[2,512]{1,0:T(2,128)(2,1)} %param.13) | copy-start | bytes 6148
  140.9 71.2 %all-gather.33.cloned.1.call-start = ((), (), s32[]{:S(2)}) async-start(), calls=%async_computation.8 | async-start | bytes 2621440 | tf_op jit(solution)/shard_map/all_gather | solution.py:41
  141.5 101.4 %all-gather.21.cloned.1.call-start = ((), (), s32[]{:S(2)}) async-start(), calls=%async_computation.2 | async-start | bytes 2359296 | tf_op jit(solution)/shard_map/all_gather | solution.py:44
  195.9 83.4 %all-gather.31.cloned.1.call-start = ((), (), s32[]{:S(2)}) async-start(), calls=%async_computation.7 | async-start | bytes 2621440 | tf_op jit(solution)/shard_map/all_gather | solution.py:40
  196.7 119.6 %all-gather.35.cloned.1.call-start = ((), (), s32[]{:S(2)}) async-start(), calls=%async_computation.9 | async-start | bytes 2621440 | tf_op jit(solution)/shard_map/all_gather | solution.py:42
  197.4 144.2 %all-gather.23.cloned.1.call-start = ((), (), s32[]{:S(2)}) async-start(), calls=%async_computation.3 | async-start | bytes 1179648 | tf_op jit(solution)/shard_map/all_gather | solution.py:71
  242.9 36.5 %copy-start.2 = (bf16[4096,256]{0,1:T(8,128)(2,1)S(1)}, bf16[4096,256]{0,1:T(8,128)(2,1)}, u32[]{:S(2)}) copy-start(bf16[4096,256]{0,1:T(8,128)(2,1)} %all-gather.21.cloned.1.call-done) | copy-start | bytes 6291460
  281.7 5.9 %collective-permute-start.3 = (bf16[256,15]{0,1:T(8,128)(2,1)S(1)}, bf16[256,15]{0,1:T(8,128)(2,1)S(1)}, u32[]{:S(2)}, u32[]{:S(2)}) collective-permute-start(bf16[256,15]{0,1:T(8,128)(2,1)S(1)} %get-tuple-element.20), channel_id=1, source_target_pairs={{8,0},{16,8},{24,16},{9,1},{17,9},{25,17},{10,2},{18,10},{26,18},{... | collective-permute-start | bytes 23048 | tf_op jit(solution)/shard_map/ppermute | solution.py:21
  283.0 5.9 %collective-permute-start.2 = (bf16[256,15]{0,1:T(8,128)(2,1)S(1)}, bf16[256,15]{0,1:T(8,128)(2,1)S(1)}, u32[]{:S(2)}, u32[]{:S(2)}) collective-permute-start(bf16[256,15]{0,1:T(8,128)(2,1)S(1)} %get-tuple-element.19), channel_id=1, source_target_pairs={{0,8},{8,16},{16,24},{1,9},{9,17},{17,25},{2,10},{10,18},{18,26},{... | collective-permute-start | bytes 23048 | tf_op jit(solution)/shard_map/ppermute | solution.py:19
  305.7 54.5 %copy-start = (bf16[512,256]{0,1:T(8,128)(2,1)S(1)}, bf16[512,256]{0,1:T(8,128)(2,1)}, u32[]{:S(2)}) copy-start(bf16[512,256]{0,1:T(8,128)(2,1)} %fusion.66) | copy-start | bytes 786436
Sparse Core Ops, SparseCore 0:
  9.2 37.8 all-gather.26
  48.7 29.1 all-gather.16
  79.7 34.5 all-gather.24
  116.0 35.0 all-gather.28
  152.5 23.8 all-gather.18
  178.2 33.9 all-gather.32
  213.7 29.1 all-gather.20
  244.8 34.5 all-gather.30
  281.2 35.0 all-gather.34
  317.7 23.8 all-gather.22
where the time goes:
time: 368 us
  waiting for transfers between devices  254 us (69%)
  blocking collectives  61.6 us (17%)
  matrix products  16.6 us (5%)
  between operations  13.8 us (4%)
  starting transfers between devices  12 us (3%)
  local copies, waits for them, and re-layouts  5.6 us (2%)
  other arithmetic  4.78 us (1%)
    all_gather x2, waiting for transfers between devices, on_device(): lax.all_gather(value_weight[layer_index], 'sp', axis=1, tiled=True)  66.4 us
    all_gather x2, waiting for transfers between devices, on_device(): block_rows = lax.all_gather(hidden, 'tp', axis=0, tiled=True)  61.6 us
    all_gather x2, waiting for transfers between devices, on_device(): lax.all_gather(activated, 'tp', axis=0, tiled=True)  50.7 us
    all_gather x2, waiting for transfers between devices, on_device(): lax.all_gather(gate_weight[layer_index], 'sp', axis=1, tiled=True)  49.7 us
    psum x2, blocking collectives, finish_layer(): square_total = lax.psum(jnp.sum(branch_wide * branch_wide, axis=0), 'tp')  31.5 us
    psum x2, blocking collectives, on_device(): lax.psum((jnp.sum(conv_wide, axis=0), jnp.sum(conv_wide * conv_wide, axis...  30.1 us
    all_gather x2, waiting for transfers between devices, on_device(): lax.all_gather(out_weight[layer_index], 'sp', axis=1, tiled=True)  19.9 us
    ppermute x2, starting transfers between devices, with_halo(): lax.ppermute(tail, axis, [(i, (i + 1) % count) for i in range(ends)])  9.09 us
  transfers between devices with their start and end apart: 14, of which 12 were waited for; matrix products, arithmetic and copies ran while one was open for 6% of the time, Pallas kernels for 0%

commit v1 on v0

--- a/solution.py
+++ b/solution.py
@@ -27,7 +27,9 @@
 
 def finish_layer(hidden, branch, feature_gain):
     branch_wide = lax.optimization_barrier(branch.astype(jnp.bfloat16)).astype(jnp.float32)
-    square_total = lax.psum(jnp.sum(branch_wide * branch_wide, axis=0), "tp")
+    part = jnp.sum(branch_wide * branch_wide, axis=0)
+    parts = lax.all_gather(part, "tp", axis=0, tiled=False)
+    square_total = parts.sum(axis=0)
     factor = lax.rsqrt(square_total / D + 1e-06)
     return (hidden.astype(jnp.float32) + branch_wide * factor * feature_gain).astype(jnp.bfloat16)
 

time: 368 us -> 363 us (0.986)
  blocking collectives: 61.6 us -> 51.6 us
  waiting for transfers between devices: 254 us -> 259 us
    psum x2 -> x0, blocking collectives: 31.5 us -> none  [finish_layer(): square_total = lax.psum(jnp.sum(branch_wide * branch_wide, axis=0), 'tp')]
    all_gather x0 -> x2, blocking collectives: none -> 21.5 us  [finish_layer(): parts = lax.all_gather(part, 'tp', axis=0, tiled=False)]
    all_gather x2, waiting for transfers between devices: 49.7 us -> 54.6 us  [on_device(): lax.all_gather(gate_weight[layer_index], 'sp', axis=1, tiled=True)]
where the time goes in v1:
time: 363 us
  waiting for transfers between devices  259 us (71%)
  blocking collectives  51.6 us (14%)
  matrix products  16.6 us (5%)
  between operations  13.8 us (4%)
  starting transfers between devices  12 us (3%)
  local copies, waits for them, and re-layouts  5.6 us (2%)
  other arithmetic  4.84 us (1%)
    all_gather x2, waiting for transfers between devices, on_device(): lax.all_gather(value_weight[layer_index], 'sp', axis=1, tiled=True)  66.4 us
    all_gather x2, waiting for transfers between devices, on_device(): block_rows = lax.all_gather(hidden, 'tp', axis=0, tiled=True)  61.6 us
    all_gather x2, waiting for transfers between devices, on_device(): lax.all_gather(gate_weight[layer_index], 'sp', axis=1, tiled=True)  54.6 us
    all_gather x2, waiting for transfers between devices, on_device(): lax.all_gather(activated, 'tp', axis=0, tiled=True)  50.7 us
    psum x2, blocking collectives, on_device(): lax.psum((jnp.sum(conv_wide, axis=0), jnp.sum(conv_wide * conv_wide, axis...  30.1 us
    all_gather x2, blocking collectives, finish_layer(): parts = lax.all_gather(part, 'tp', axis=0, tiled=False)  21.5 us
    all_gather x2, waiting for transfers between devices, on_device(): lax.all_gather(out_weight[layer_index], 'sp', axis=1, tiled=True)  19.9 us
    ppermute x2, starting transfers between devices, with_halo(): lax.ppermute(tail, axis, [(i, (i + 1) % count) for i in range(ends)])  9.09 us
  transfers between devices with their start and end apart: 14, of which 12 were waited for; matrix products, arithmetic and copies ran while one was open for 6% of the time, Pallas kernels for 0%

profile of v1, /device:TPU:0, one launch (start us, length us, event | category | flops | bytes accessed | tf_op | source)
XLA Modules:
  0.0 363.0 jit_solution(18314734911827368086)
XLA Ops:
  6.5 2.4 fusion.155
  9.7 1.0 fusion.154
  10.8 1.1 fusion.153
  12.1 35.0 %all-gather.31.cloned.1.call-done = bf16[1,256,4096]{2,1,0:T(8,128)(2,1)} async-done(((bf16[1,256,1024]{2,1,0:T(8,128)(2,1)}), bf16[1,256,4096]{2,1,0:T(8,128)(2,1)}) %all-gather.31.cloned.1.call-update) | async-done | bytes 2097168 | tf_op jit(solution)/shard_map/all_gather | solution.py:43
  47.1 30.8 %all-gather.21.cloned.1.call-done = bf16[4096,256]{1,0:T(8,128)(2,1)} async-done(((bf16[512,256]{1,0:T(8,128)(2,1)}), bf16[4096,256]{1,0:T(8,128)(2,1)}) %all-gather.21.cloned.1.call-update) | async-done | bytes 2097168 | tf_op jit(solution)/shard_map/all_gather | solution.py:46
  77.9 3.3 fusion.36
  81.2 33.1 %all-gather.29.cloned.1.call-done = bf16[1,256,4096]{2,1,0:T(8,128)(2,1)} async-done(((bf16[1,256,1024]{2,1,0:T(8,128)(2,1)}), bf16[1,256,4096]{2,1,0:T(8,128)(2,1)}) %all-gather.29.cloned.1.call-update) | async-done | bytes 2097168 | tf_op jit(solution)/shard_map/all_gather | solution.py:42
  114.4 2.5 fusion.57
  116.9 1.3 collective-permute-start.1
  118.2 4.5 %collective-permute-start = (bf16[256,15]{0,1:T(8,128)(2,1)S(1)}, bf16[256,15]{0,1:T(8,128)(2,1)S(1)}, u32[]{:S(2)}, u32[]{:S(2)}) collective-permute-start(bf16[256,15]{0,1:T(8,128)(2,1)S(1)} %get-tuple-element.21), channel_id=1, source_target_pairs={{0,8},{8,16},{16,24},{1,9},{9,17},{17,25},{2,10},{10,18},{18,26},{... | collective-permute-start | bytes 23048 | tf_op jit(solution)/shard_map/ppermute | solution.py:19
  122.8 1.3 collective-permute-done
  125.0 15.1 %all-reduce.1 = (f32[256]{0:T(256)S(1)}, f32[256]{0:T(256)S(1)}) all-reduce(f32[256]{0:T(256)S(1)} %get-tuple-element.8, f32[256]{0:T(256)S(1)} %get-tuple-element.7), channel_id=1, replica_groups=mesh['sp'=4,'tp'=8] {'tp'}, use_global_device_ids=true, to_apply=%region_3.0 | all-reduce | flops 512 | bytes 4096 | tf_op jit(solution)/shard_map/psum | solution.py:62
  140.1 0.8 fusion.78
  141.7 9.4 %all-gather.33.cloned.1.call-done = bf16[1,512,2048]{2,1,0:T(8,128)(2,1)} async-done(((bf16[1,512,512]{2,1,0:T(8,128)(2,1)}), bf16[1,512,2048]{2,1,0:T(8,128)(2,1)}) %all-gather.33.cloned.1.call-update) | async-done | bytes 2097168 | tf_op jit(solution)/shard_map/all_gather | solution.py:44
  151.1 25.3 %all-gather.23.cloned.1.call-done = bf16[2048,256]{0,1:T(8,128)(2,1)} async-done(((bf16[256,256]{0,1:T(8,128)(2,1)}), bf16[2048,256]{0,1:T(8,128)(2,1)}) %all-gather.23.cloned.1.call-update) | async-done | bytes 1048592 | tf_op jit(solution)/shard_map/all_gather | solution.py:73
  176.5 2.7 fusion.21
  179.3 10.7 %all-gather.8 = f32[8,1,256]{2,1,0:T(1,128)S(1)} all-gather(f32[1,1,256]{2,1,0:T(1,128)S(1)} %bitcast.144), channel_id=5, replica_groups=mesh['sp'=4,'tp'=8] {'tp'}, dimensions={0}, use_global_device_ids=true | all-gather | bytes 9216 | tf_op jit(solution)/shard_map/all_gather | solution.py:31
  190.0 0.9 fusion.66
  192.5 19.6 %all-gather.37.cloned.1.call-done = bf16[1,256,4096]{2,1,0:T(8,128)(2,1)} async-done(((bf16[1,256,1024]{2,1,0:T(8,128)(2,1)}), bf16[1,256,4096]{2,1,0:T(8,128)(2,1)}) %all-gather.37.cloned.1.call-update) | async-done | bytes 2097168 | tf_op jit(solution)/shard_map/all_gather | solution.py:43
  212.1 30.8 %all-gather.25.cloned.1.call-done = bf16[4096,256]{0,1:T(8,128)(2,1)} async-done(((bf16[512,256]{0,1:T(8,128)(2,1)}), bf16[4096,256]{0,1:T(8,128)(2,1)}) %all-gather.25.cloned.1.call-update) | async-done | bytes 2097168 | tf_op jit(solution)/shard_map/all_gather | solution.py:46
  242.9 3.1 fusion.51
  246.0 33.3 %all-gather.35.cloned.1.call-done = bf16[1,256,4096]{2,1,0:T(8,128)(2,1)} async-done(((bf16[1,256,1024]{2,1,0:T(8,128)(2,1)}), bf16[1,256,4096]{2,1,0:T(8,128)(2,1)}) %all-gather.35.cloned.1.call-update) | async-done | bytes 2097168 | tf_op jit(solution)/shard_map/all_gather | solution.py:42
  279.4 2.3 fusion.60
  281.7 1.3 collective-permute-start.3
  283.0 4.5 %collective-permute-start.2 = (bf16[256,15]{0,1:T(8,128)(2,1)S(1)}, bf16[256,15]{0,1:T(8,128)(2,1)S(1)}, u32[]{:S(2)}, u32[]{:S(2)}) collective-permute-start(bf16[256,15]{0,1:T(8,128)(2,1)S(1)} %get-tuple-element.19), channel_id=1, source_target_pairs={{0,8},{8,16},{16,24},{1,9},{9,17},{17,25},{2,10},{10,18},{18,26},{... | collective-permute-start | bytes 23048 | tf_op jit(solution)/shard_map/ppermute | solution.py:19
  287.6 1.3 collective-permute-done.2
  289.8 15.1 %all-reduce = (f32[256]{0:T(256)S(1)}, f32[256]{0:T(256)S(1)}) all-reduce(f32[256]{0:T(256)S(1)} %get-tuple-element.6, f32[256]{0:T(256)S(1)} %get-tuple-element.5), channel_id=1, replica_groups=mesh['sp'=4,'tp'=8] {'tp'}, use_global_device_ids=true, to_apply=%region_9.10 | all-reduce | flops 512 | bytes 4096 | tf_op jit(solution)/shard_map/psum | solution.py:62
  304.9 0.8 fusion.87
  305.7 10.5 %all-gather.39.cloned.1.call-done = bf16[1,512,2048]{2,1,0:T(8,128)(2,1)} async-done(((bf16[1,512,512]{2,1,0:T(8,128)(2,1)}), bf16[1,512,2048]{2,1,0:T(8,128)(2,1)}) %all-gather.39.cloned.1.call-update) | async-done | bytes 2097168 | tf_op jit(solution)/shard_map/all_gather | solution.py:44
  316.3 25.3 %all-gather.27.cloned.1.call-done = bf16[2048,256]{0,1:T(8,128)(2,1)} async-done(((bf16[256,256]{0,1:T(8,128)(2,1)}), bf16[2048,256]{0,1:T(8,128)(2,1)}) %all-gather.27.cloned.1.call-update) | async-done | bytes 1048592 | tf_op jit(solution)/shard_map/all_gather | solution.py:73
  341.6 2.7 fusion.18
  344.4 10.7 %all-gather.9 = f32[8,1,256]{2,1,0:T(1,128)S(1)} all-gather(f32[1,1,256]{2,1,0:T(1,128)S(1)} %bitcast.145), channel_id=9, replica_groups=mesh['sp'=4,'tp'=8] {'tp'}, dimensions={0}, use_global_device_ids=true | all-gather | bytes 9216 | tf_op jit(solution)/shard_map/all_gather | solution.py:31
  (67 shorter events, 6.5 us)
Async XLA Ops:
  6.5 3.2 copy-start.3
  6.5 40.6 %all-gather.31.cloned.1.call-start = ((), (), s32[]{:S(2)}) async-start(), calls=%async_computation.5 | async-start | bytes 2621440 | tf_op jit(solution)/shard_map/all_gather | solution.py:43
  8.9 1.9 copy-start.4
  8.9 69.0 %all-gather.21.cloned.1.call-start = ((), (), s32[]{:S(2)}) async-start(), calls=%async_computation | async-start | bytes 2359296 | tf_op jit(solution)/shard_map/all_gather | solution.py:46
  9.7 104.7 %all-gather.29.cloned.1.call-start = ((), (), s32[]{:S(2)}) async-start(), calls=%async_computation.4 | async-start | bytes 2621440 | tf_op jit(solution)/shard_map/all_gather | solution.py:42
  10.8 1.2 copy-start.6
  10.8 140.3 %all-gather.33.cloned.1.call-start = ((), (), s32[]{:S(2)}) async-start(), calls=%async_computation.6 | async-start | bytes 2621440 | tf_op jit(solution)/shard_map/all_gather | solution.py:44
  11.9 164.5 %all-gather.23.cloned.1.call-start = ((), (), s32[]{:S(2)}) async-start(), calls=%async_computation.1 | async-start | bytes 1179648 | tf_op jit(solution)/shard_map/all_gather | solution.py:73
  77.9 36.5 %copy-start.1 = (bf16[4096,256]{1,0:T(8,128)(2,1)S(1)}, bf16[4096,256]{1,0:T(8,128)(2,1)}, u32[]{:S(2)}) copy-start(bf16[4096,256]{1,0:T(8,128)(2,1)} %all-gather.21.cloned.1.call-done) | copy-start | bytes 6291460
  81.2 41.5 %copy-start.8 = (bf16[2,256]{1,0:T(2,128)(2,1)S(1)}, bf16[2,256]{1,0:T(2,128)(2,1)}, u32[]{:S(2)}) copy-start(bf16[2,256]{1,0:T(2,128)(2,1)} %param.11) | copy-start | bytes 3076
  116.9 5.9 %collective-permute-start.1 = (bf16[256,15]{0,1:T(8,128)(2,1)S(1)}, bf16[256,15]{0,1:T(8,128)(2,1)S(1)}, u32[]{:S(2)}, u32[]{:S(2)}) collective-permute-start(bf16[256,15]{0,1:T(8,128)(2,1)S(1)} %get-tuple-element.22), channel_id=1, source_target_pairs={{8,0},{16,8},{24,16},{9,1},{17,9},{25,17},{10,2},{18,10},{26,18},{... | collective-permute-start | bytes 23048 | tf_op jit(solution)/shard_map/ppermute | solution.py:21
  118.2 5.9 %collective-permute-start = (bf16[256,15]{0,1:T(8,128)(2,1)S(1)}, bf16[256,15]{0,1:T(8,128)(2,1)S(1)}, u32[]{:S(2)}, u32[]{:S(2)}) collective-permute-start(bf16[256,15]{0,1:T(8,128)(2,1)S(1)} %get-tuple-element.21), channel_id=1, source_target_pairs={{0,8},{8,16},{16,24},{1,9},{9,17},{17,25},{2,10},{10,18},{18,26},{... | collective-permute-start | bytes 23048 | tf_op jit(solution)/shard_map/ppermute | solution.py:19
  124.1 17.4 %copy-start.5 = (bf16[512,256]{1,0:T(8,128)(2,1)S(1)}, bf16[512,256]{1,0:T(8,128)(2,1)}, u32[]{:S(2)}) copy-start(bf16[512,256]{1,0:T(8,128)(2,1)} %param.7) | copy-start | bytes 786436
  124.1 17.6 %copy-start.7 = (bf16[2,512]{1,0:T(2,128)(2,1)S(1)}, bf16[2,512]{1,0:T(2,128)(2,1)}, u32[]{:S(2)}) copy-start(bf16[2,512]{1,0:T(2,128)(2,1)} %param.13) | copy-start | bytes 6148
  140.9 71.2 %all-gather.37.cloned.1.call-start = ((), (), s32[]{:S(2)}) async-start(), calls=%async_computation.8 | async-start | bytes 2621440 | tf_op jit(solution)/shard_map/all_gather | solution.py:43
  141.5 101.4 %all-gather.25.cloned.1.call-start = ((), (), s32[]{:S(2)}) async-start(), calls=%async_computation.2 | async-start | bytes 2359296 | tf_op jit(solution)/shard_map/all_gather | solution.py:46
  190.9 88.4 %all-gather.35.cloned.1.call-start = ((), (), s32[]{:S(2)}) async-start(), calls=%async_computation.7 | async-start | bytes 2621440 | tf_op jit(solution)/shard_map/all_gather | solution.py:42
  191.7 124.6 %all-gather.39.cloned.1.call-start = ((), (), s32[]{:S(2)}) async-start(), calls=%async_computation.9 | async-start | bytes 2621440 | tf_op jit(solution)/shard_map/all_gather | solution.py:44
  192.4 149.2 %all-gather.27.cloned.1.call-start = ((), (), s32[]{:S(2)}) async-start(), calls=%async_computation.3 | async-start | bytes 1179648 | tf_op jit(solution)/shard_map/all_gather | solution.py:73
  242.9 36.4 %copy-start.2 = (bf16[4096,256]{0,1:T(8,128)(2,1)S(1)}, bf16[4096,256]{0,1:T(8,128)(2,1)}, u32[]{:S(2)}) copy-start(bf16[4096,256]{0,1:T(8,128)(2,1)} %all-gather.25.cloned.1.call-done) | copy-start | bytes 6291460
  281.7 5.9 %collective-permute-start.3 = (bf16[256,15]{0,1:T(8,128)(2,1)S(1)}, bf16[256,15]{0,1:T(8,128)(2,1)S(1)}, u32[]{:S(2)}, u32[]{:S(2)}) collective-permute-start(bf16[256,15]{0,1:T(8,128)(2,1)S(1)} %get-tuple-element.20), channel_id=1, source_target_pairs={{8,0},{16,8},{24,16},{9,1},{17,9},{25,17},{10,2},{18,10},{26,18},{... | collective-permute-start | bytes 23048 | tf_op jit(solution)/shard_map/ppermute | solution.py:21
  283.0 5.9 %collective-permute-start.2 = (bf16[256,15]{0,1:T(8,128)(2,1)S(1)}, bf16[256,15]{0,1:T(8,128)(2,1)S(1)}, u32[]{:S(2)}, u32[]{:S(2)}) collective-permute-start(bf16[256,15]{0,1:T(8,128)(2,1)S(1)} %get-tuple-element.19), channel_id=1, source_target_pairs={{0,8},{8,16},{16,24},{1,9},{9,17},{17,25},{2,10},{10,18},{18,26},{... | collective-permute-start | bytes 23048 | tf_op jit(solution)/shard_map/ppermute | solution.py:19
  305.7 49.5 %copy-start = (bf16[512,256]{0,1:T(8,128)(2,1)S(1)}, bf16[512,256]{0,1:T(8,128)(2,1)}, u32[]{:S(2)}) copy-start(bf16[512,256]{0,1:T(8,128)(2,1)} %fusion.66) | copy-start | bytes 786436
Sparse Core Ops, SparseCore 0:
  9.2 37.8 all-gather.30
  48.7 29.1 all-gather.20
  79.7 34.5 all-gather.28
  116.0 35.0 all-gather.32
  152.5 23.8 all-gather.22
  178.2 33.9 all-gather.36
  213.7 29.1 all-gather.24
  244.8 34.5 all-gather.34
  281.2 35.0 all-gather.38
  317.7 23.8 all-gather.26
